TPU v7x, 32 devices: a whole 2x2x4 slice. The times are simulated.
32 devices in a mesh: fs: 8 (over z, x), tp: 4 (over y, core).
Axes of the slice: x: 2, y: 2, z: 4, core: 2. Of those that a mesh axis runs over, the one named last changes fastest.
Arguments:
- tokens: bfloat16 [4096, 2048], P(('fs', 'tp')), may hold values from -6 to 6
- gate_weight: bfloat16 [2048, 6144], P('fs', 'tp'), may hold values from -0.125 to 0.125
- value_weight: bfloat16 [2048, 6144], P('fs', 'tp'), may hold values from -0.125 to 0.125
- gate_taps: float32 [3, 6144], P(None, 'tp'), may hold values from -3.5 to 3.5
- value_taps: float32 [3, 6144], P(None, 'tp'), may hold values from -3.5 to 3.5
- down_weight: bfloat16 [6144, 2048], P('tp', 'fs'), may hold values from -0.078125 to 0.078125
- norm_gain: float32 [2048], replicated, may hold values from 0.1 to 1.9
- norm_shift: float32 [2048], replicated, may hold values from -3 to 3
Outputs:
- mixed: bfloat16 [4096, 2048], P(('fs', 'tp'))
All inputs are finite; a program needn't handle non-finite values.
Results may differ from a plain program's by a relative error of at most 0.017.
Values may be sent and summed in bfloat16 or wider, within the bound.
A program may use at most 256 MiB of HBM per device.

v0:
```python
import jax
import jax.numpy as jnp
from jax import lax
from jax.sharding import PartitionSpec as P


def causal_mix(pre, kernel_taps):
    leading = jnp.zeros((2, pre.shape[1]), jnp.float32)
    padded = jnp.concatenate([leading, pre.astype(jnp.float32)], axis=0)
    length = pre.shape[0]
    return (
        kernel_taps[0] * padded[0:length]
        + kernel_taps[1] * padded[1 : length + 1]
        + kernel_taps[2] * padded[2 : length + 2]
    )


def local(
    tokens, gate_weight, value_weight, gate_taps, value_taps, down_weight, norm_gain, norm_shift
):
    sequence = lax.all_gather(tokens, "tp", axis=0, tiled=True)

    def add_rows(segment):
        return jnp.dot(sequence, segment, preferred_element_type=jnp.float32)

    gate_sum = add_rows(lax.all_gather(gate_weight, "fs", axis=0, tiled=True))
    value_sum = add_rows(lax.all_gather(value_weight, "fs", axis=0, tiled=True))
    gate_mix = causal_mix(gate_sum.astype(jnp.bfloat16), gate_taps)
    value_mix = causal_mix(value_sum.astype(jnp.bfloat16), value_taps)
    hidden = (jax.nn.gelu(gate_mix, approximate=False) * value_mix).astype(jnp.bfloat16)
    partial_terms = jnp.dot(
        hidden,
        lax.all_gather(down_weight, "fs", axis=1, tiled=True),
        preferred_element_type=jnp.float32,
    )
    summed = lax.psum_scatter(
        partial_terms.astype(jnp.bfloat16), "tp", scatter_dimension=0, tiled=True
    ).astype(jnp.float32)
    average = jnp.mean(summed, axis=1, keepdims=True)
    centered = summed - average
    variance = jnp.mean(centered * centered, axis=1, keepdims=True)
    normed = centered * lax.rsqrt(variance + 1e-05) * norm_gain + norm_shift
    return normed.astype(jnp.bfloat16)


def solution(mesh):
    in_specs = (
        P(("fs", "tp"), None),
        P("fs", "tp"),
        P("fs", "tp"),
        P(None, "tp"),
        P(None, "tp"),
        P("tp", "fs"),
        P(),
        P(),
    )
    out_specs = P(("fs", "tp"), None)
    return jax.shard_map(local, mesh=mesh, in_specs=in_specs, out_specs=out_specs, check_vma=False)
```

profile of v0, /device:TPU:0, one launch (start us, length us, event | category | flops | bytes accessed | tf_op | source)
XLA Modules:
  0.0 394.9 jit_solution(5087503630397722218)
XLA Ops:
  6.5 0.0 all-gather.5.cloned.1.call-start
  6.5 0.7 all-gather.5.cloned.1.call-update
  7.3 0.0 all-gather.7.cloned.1.call-start
  7.3 0.7 all-gather.7.cloned.1.call-update
  8.0 0.0 all-gather.9.cloned.1.call-start
  8.1 0.7 all-gather.9.cloned.1.call-update
  8.7 0.0 all-gather.11.cloned.1.call-start
  8.8 0.5 all-gather.11.cloned.1.call-update
  9.3 0.0 reduce-scatter.2.cloned.1.call-start
  9.4 1.0 slice_reduce_fusion.2
  10.3 23.9 %all-gather.5.cloned.1.call-done = bf16[512,2048]{1,0:T(8,128)(2,1)} async-done(((bf16[128,2048]{1,0:T(8,128)(2,1)}), bf16[512,2048]{1,0:T(8,128)(2,1)}) %all-gather.5.cloned.1.call-update) | async-done | bytes 2097168 | tf_op jit(solution)/shard_map/all_gather | solution.py:21
  34.2 0.0 copy-start.2
  34.2 100.9 %all-gather.7.cloned.1.call-done = bf16[2048,1536]{1,0:T(8,128)(2,1)} async-done(((bf16[256,1536]{1,0:T(8,128)(2,1)}), bf16[2048,1536]{1,0:T(8,128)(2,1)}) %all-gather.7.cloned.1.call-update) | async-done | bytes 6291472 | tf_op jit(solution)/shard_map/all_gather | solution.py:26
  135.1 8.5 %fusion.12 = f32[512,1536]{1,0:T(8,128)} fusion(bf16[512,2048]{1,0:T(8,128)(2,1)} %all-gather.5.cloned.1.call-done, bf16[2048,1536]{1,0:T(8,128)(2,1)} %all-gather.7.cloned.1.call-done), kind=kOutput, calls=%fused_computation.25 | convolution fusion | flops 3222798336 | bytes 11534336 | tf_op jit(solution)/shard_map/dot_general | solution.py:24
  143.6 90.6 %all-gather.9.cloned.1.call-done = bf16[2048,1536]{1,0:T(8,128)(2,1)} async-done(((bf16[256,1536]{1,0:T(8,128)(2,1)}), bf16[2048,1536]{1,0:T(8,128)(2,1)}) %all-gather.9.cloned.1.call-update) | async-done | bytes 6291472 | tf_op jit(solution)/shard_map/all_gather | solution.py:27
  234.2 0.0 copy-done.2
  234.2 7.9 %fusion.11 = f32[512,1536]{1,0:T(8,128)} fusion(bf16[512,2048]{1,0:T(8,128)(2,1)S(1)} %copy-done.2, bf16[2048,1536]{1,0:T(8,128)(2,1)} %all-gather.9.cloned.1.call-done), kind=kOutput, calls=%fused_computation.23 | convolution fusion | flops 3222798336 | bytes 11534336 | tf_op jit(solution)/shard_map/dot_general | solution.py:24
  242.1 91.7 %all-gather.11.cloned.1.call-done = bf16[1536,2048]{1,0:T(8,128)(2,1)} async-done(((bf16[1536,256]{1,0:T(8,128)(2,1)}), bf16[1536,2048]{1,0:T(8,128)(2,1)}) %all-gather.11.cloned.1.call-update) | async-done | bytes 6291472 | tf_op jit(solution)/shard_map/all_gather | solution.py:33
  333.8 20.2 %convolution_convert_fusion = bf16[512,2048]{1,0:T(8,128)(2,1)} fusion(bf16[1536,2048]{1,0:T(8,128)(2,1)} %all-gather.11.cloned.1.call-done, f32[512,1536]{1,0:T(8,128)} %fusion.11, f32[512,1536]{1,0:T(8,128)} %fusion.12, f32[1536]{0:T(1024)S(1)} %get-tuple-element.9, f32[1536]{0:T(1024)S(1)} %get-tuple-element.10, f32[1536]{0:T(1024)S(1)} %get-tuple-element.8, ...), kind=kOutput, calls=%fused_computation.21 | convolution fusion | flops 3282042880 | bytes 14716928 | tf_op jit(solution)/shard_map/dot_general | solution.py:31
  354.0 0.0 copy-start
  354.0 0.0 copy-start.1
  354.0 0.0 reduce-scatter.2.cloned.1.call-update
  354.1 29.5 %reduce-scatter.2.cloned.1.call-done = bf16[128,2048]{1,0:T(8,128)(2,1)} async-done(((bf16[512,2048]{1,0:T(8,128)(2,1)}), bf16[128,2048]{1,0:T(8,128)(2,1)}) %reduce-scatter.2.cloned.1.call-update) | async-done | bytes 524304 | tf_op jit(solution)/shard_map/reduce_scatter | solution.py:36
  383.6 1.2 convert_reduce_fusion
  384.8 1.3 fusion.16
  386.1 0.0 copy-done
  386.1 0.0 copy-done.1
  386.1 2.2 fusion.19
  (2 shorter events, 0.0 us)
Async XLA Ops:
  6.5 27.7 %all-gather.5.cloned.1.call-start = ((), (), s32[]{:S(2)}) async-start(), calls=%async_computation.1 | async-start | bytes 2621440 | tf_op jit(solution)/shard_map/all_gather | solution.py:21
  7.3 127.9 %all-gather.7.cloned.1.call-start = ((), (), s32[]{:S(2)}) async-start(), calls=%async_computation.2 | async-start | bytes 7077888 | tf_op jit(solution)/shard_map/all_gather | solution.py:26
  8.0 226.2 %all-gather.9.cloned.1.call-start = ((), (), s32[]{:S(2)}) async-start(), calls=%async_computation.3 | async-start | bytes 7077888 | tf_op jit(solution)/shard_map/all_gather | solution.py:27
  8.7 325.1 %all-gather.11.cloned.1.call-start = ((), (), s32[]{:S(2)}) async-start(), calls=%async_computation.4 | async-start | bytes 7077888 | tf_op jit(solution)/shard_map/all_gather | solution.py:33
  9.3 374.3 %reduce-scatter.2.cloned.1.call-start = ((), (), s32[]{:S(2)}) async-start(), calls=%async_computation.5 | async-start | bytes 2621440 | tf_op jit(solution)/shard_map/reduce_scatter | solution.py:36
  34.2 200.0 %copy-start.2 = (bf16[512,2048]{1,0:T(8,128)(2,1)S(1)}, bf16[512,2048]{1,0:T(8,128)(2,1)}, u32[]{:S(2)}) copy-start(bf16[512,2048]{1,0:T(8,128)(2,1)} %all-gather.5.cloned.1.call-done) | copy-start | bytes 6291460
  354.0 32.1 %copy-start = (f32[2048]{0:T(1024)S(1)}, f32[2048]{0:T(1024)}, u32[]{:S(2)}) copy-start(f32[2048]{0:T(1024)} %param.15) | copy-start | bytes 24580
  354.0 32.1 %copy-start.1 = (f32[2048]{0:T(1024)S(1)}, f32[2048]{0:T(1024)}, u32[]{:S(2)}) copy-start(f32[2048]{0:T(1024)} %param.14) | copy-start | bytes 24580
Sparse Core Ops, SparseCore 0:
  8.9 25.2 all-gather.4
  36.4 98.6 all-gather.6
  137.3 96.8 all-gather.8
  236.1 97.6 all-gather.10
  354.2 29.3 reduce-scatter.1
where the time goes:
time: 395 us
  waiting for transfers between devices  339 us (86%)
  matrix products  36.6 us (9%)
  between operations  13.2 us (3%)
  other arithmetic  4.78 us (1%)
    all_gather x1, waiting for transfers between devices, local(): gate_sum = add_rows(lax.all_gather(gate_weight, 'fs', axis=0, tiled=True))  101 us
    all_gather x1, waiting for transfers between devices, local(): lax.all_gather(down_weight, 'fs', axis=1, tiled=True)  91.7 us
    all_gather x1, waiting for transfers between devices, local(): value_sum = add_rows(lax.all_gather(value_weight, 'fs', axis=0, tiled=True))  90.6 us
    reduce_scatter x1, waiting for transfers between devices, local(): lax.psum_scatter(partial_terms.astype(jnp.bfloat16), 'tp', scatter_dimens...  29.5 us
    all_gather x1, waiting for transfers between devices, local(): sequence = lax.all_gather(tokens, 'tp', axis=0, tiled=True)  23.9 us
    dot_general x1, matrix products, local(): jnp.dot(hidden, lax.all_gather(down_weight, 'fs', axis=1, tiled=True), pr...  20.2 us
    dot_general x2, matrix products, add_rows(): return jnp.dot(sequence, segment, preferred_element_type=jnp.float32)  16.4 us
  transfers between devices with their start and end apart: 5, of which 5 were waited for; matrix products, arithmetic and copies ran while one was open for 4% of the time, Pallas kernels for 0%

commit v1 on v0

--- a/solution.py
+++ b/solution.py
@@ -2,6 +2,16 @@
 import jax.numpy as jnp
 from jax import lax
 from jax.sharding import PartitionSpec as P
+
+
+def pass_along(x, axis, dim):
+    n_dev = lax.axis_size(axis)
+    current, blocks = (x, [x])
+    for _ in range(n_dev - 1):
+        current = lax.ppermute(current, axis, [(i, (i + 1) % n_dev) for i in range(n_dev)])
+        blocks.insert(0, current)
+    line = jnp.concatenate(blocks, axis=dim)
+    return jnp.roll(line, (lax.axis_index(axis) + 1) * x.shape[dim], axis=dim)
 
 
 def causal_mix(pre, kernel_taps):
@@ -18,7 +28,7 @@
 def local(
     tokens, gate_weight, value_weight, gate_taps, value_taps, down_weight, norm_gain, norm_shift
 ):
-    sequence = lax.all_gather(tokens, "tp", axis=0, tiled=True)
+    sequence = pass_along(tokens, "tp", 0)
 
     def add_rows(segment):
         return jnp.dot(sequence, segment, preferred_element_type=jnp.float32)

time: 395 us -> 372 us (0.942)
  waiting for transfers between devices: 339 us -> 307 us
  local copies, waits for them, and re-layouts: 0.99 us -> 7.72 us
    all_gather x1, waiting for transfers between devices: 101 us -> 68.6 us  [local(): gate_sum = add_rows(lax.all_gather(gate_weight, 'fs', axis=0, tiled=True))]
    ppermute x0 -> x3, waiting for transfers between devices: none -> 25.2 us  [pass_along(): lax.ppermute(current, axis, [(i, (i + 1) % n_dev) for i in range(n_dev)])]
    all_gather x1 -> x0, waiting for transfers between devices: 23.9 us -> none  [local(): sequence = lax.all_gather(tokens, 'tp', axis=0, tiled=True)]
    unnamed x6 -> x13, local copies, waits for them, and re-layouts: 0.01 us -> 5.9 us
  transfers between devices with their start and end apart: 5 -> 7, of which waited for: 5 -> 7; matrix products, arithmetic and copies ran while one was open for 4% -> 7% of each run, Pallas kernels for 0% -> 0%
where the time goes in v1:
time: 372 us; the launch traced here: 371 us
  waiting for transfers between devices  307 us (83%)
  matrix products  37.6 us (10%)
  between operations  13.2 us (4%)
  local copies, waits for them, and re-layouts  7.72 us (2%)
  other arithmetic  4.78 us (1%)
    all_gather x1, waiting for transfers between devices, local(): lax.all_gather(down_weight, 'fs', axis=1, tiled=True)  91.2 us
    all_gather x1, waiting for transfers between devices, local(): value_sum = add_rows(lax.all_gather(value_weight, 'fs', axis=0, tiled=True))  90.6 us
    all_gather x1, waiting for transfers between devices, local(): gate_sum = add_rows(lax.all_gather(gate_weight, 'fs', axis=0, tiled=True))  68.6 us
    reduce_scatter x1, waiting for transfers between devices, local(): lax.psum_scatter(partial_terms.astype(jnp.bfloat16), 'tp', scatter_dimens...  29.5 us
    ppermute x3, waiting for transfers between devices, pass_along(): lax.ppermute(current, axis, [(i, (i + 1) % n_dev) for i in range(n_dev)])  25.2 us
    dot_general x1, matrix products, local(): jnp.dot(hidden, lax.all_gather(down_weight, 'fs', axis=1, tiled=True), pr...  20.5 us
    dot_general x2, matrix products, add_rows(): return jnp.dot(sequence, segment, preferred_element_type=jnp.float32)  17 us
  transfers between devices with their start and end apart: 7, of which 7 were waited for; matrix products, arithmetic and copies ran while one was open for 7% of the time, Pallas kernels for 0%

profile of v1, /device:TPU:0, one launch (start us, length us, event | category | flops | bytes accessed | tf_op | source)
XLA Modules:
  0.0 371.2 jit_solution(5005801571992568753)
XLA Ops:
  6.5 0.7 all-gather.4.cloned.1.call-update
  7.3 0.0 all-gather.6.cloned.1.call-start
  7.3 0.7 all-gather.6.cloned.1.call-update
  8.0 0.0 all-gather.8.cloned.1.call-start
  8.1 0.7 all-gather.8.cloned.1.call-update
  8.7 0.0 reduce-scatter.2.cloned.1.call-start
  8.8 0.5 collective-permute-start
  9.3 9.0 %collective-permute-done = bf16[128,2048]{1,0:T(8,128)(2,1)S(1)} collective-permute-done((bf16[128,2048]{1,0:T(8,128)(2,1)}, bf16[128,2048]{1,0:T(8,128)(2,1)S(1)}, u32[]{:S(2)}, u32[]{:S(2)}) %collective-permute-start) | collective-permute-done | bytes 524320 | tf_op jit(solution)/shard_map/ppermute | solution.py:11
  18.4 0.0 collective-permute-start.1
  18.4 8.6 %collective-permute-done.1 = bf16[128,2048]{1,0:T(8,128)(2,1)S(1)} collective-permute-done((bf16[128,2048]{1,0:T(8,128)(2,1)S(1)}, bf16[128,2048]{1,0:T(8,128)(2,1)S(1)}, u32[]{:S(2)}, u32[]{:S(2)}) %collective-permute-start.1) | collective-permute-done | bytes 524320 | tf_op jit(solution)/shard_map/ppermute | solution.py:11
  27.0 0.0 collective-permute-start.2
  27.0 1.0 slice_reduce_fusion.2
  27.9 7.6 %collective-permute-done.2 = bf16[128,2048]{1,0:T(8,128)(2,1)S(1)} collective-permute-done((bf16[128,2048]{1,0:T(8,128)(2,1)S(1)}, bf16[128,2048]{1,0:T(8,128)(2,1)S(1)}, u32[]{:S(2)}, u32[]{:S(2)}) %collective-permute-start.2) | collective-permute-done | bytes 524320 | tf_op jit(solution)/shard_map/ppermute | solution.py:11
  35.6 0.8 constant_dynamic-update-slice_fusion.7
  36.4 0.9 constant_dynamic-update-slice_fusion.6
  37.2 0.8 constant_dynamic-update-slice_fusion.5
  38.1 0.9 constant_dynamic-update-slice_fusion.4
  38.9 0.8 constant_dynamic-update-slice_fusion.3
  39.8 0.9 constant_dynamic-update-slice_fusion.2
  40.6 0.8 constant_dynamic-update-slice_fusion.1
  41.5 0.9 constant_dynamic-update-slice_fusion
  42.3 68.6 %all-gather.4.cloned.1.call-done = bf16[2048,1536]{1,0:T(8,128)(2,1)} async-done(((bf16[256,1536]{1,0:T(8,128)(2,1)}), bf16[2048,1536]{1,0:T(8,128)(2,1)}) %all-gather.4.cloned.1.call-update) | async-done | bytes 6291472 | tf_op jit(solution)/shard_map/all_gather | solution.py:36
  111.0 8.5 %fusion.12 = f32[512,1536]{1,0:T(8,128)} fusion(bf16[2048,1536]{1,0:T(8,128)(2,1)} %all-gather.4.cloned.1.call-done, bf16[1024,2048]{1,0:T(8,128)(2,1)} %constant_dynamic-update-slice_fusion, s32[]{:T(128)S(6)} %select_n.14), kind=kOutput, calls=%fused_computation.25 | convolution fusion | flops 3222798336 | bytes 11534340 | tf_op jit(solution)/shard_map/dot_general | solution.py:34
  119.5 90.6 %all-gather.6.cloned.1.call-done = bf16[2048,1536]{1,0:T(8,128)(2,1)} async-done(((bf16[256,1536]{1,0:T(8,128)(2,1)}), bf16[2048,1536]{1,0:T(8,128)(2,1)}) %all-gather.6.cloned.1.call-update) | async-done | bytes 6291472 | tf_op jit(solution)/shard_map/all_gather | solution.py:37
  210.1 8.5 %fusion.11 = f32[512,1536]{1,0:T(8,128)} fusion(bf16[2048,1536]{1,0:T(8,128)(2,1)} %all-gather.6.cloned.1.call-done, bf16[1024,2048]{1,0:T(8,128)(2,1)} %constant_dynamic-update-slice_fusion, s32[]{:T(128)S(6)} %select_n.14), kind=kOutput, calls=%fused_computation.23 | convolution fusion | flops 3222798336 | bytes 11534340 | tf_op jit(solution)/shard_map/dot_general | solution.py:34
  218.6 91.2 %all-gather.8.cloned.1.call-done = bf16[1536,2048]{1,0:T(8,128)(2,1)} async-done(((bf16[1536,256]{1,0:T(8,128)(2,1)}), bf16[1536,2048]{1,0:T(8,128)(2,1)}) %all-gather.8.cloned.1.call-update) | async-done | bytes 6291472 | tf_op jit(solution)/shard_map/all_gather | solution.py:43
  309.8 20.5 %convolution_convert_fusion = bf16[512,2048]{1,0:T(8,128)(2,1)} fusion(bf16[1536,2048]{1,0:T(8,128)(2,1)} %all-gather.8.cloned.1.call-done, f32[512,1536]{1,0:T(8,128)} %fusion.11, f32[512,1536]{1,0:T(8,128)} %fusion.12, f32[1536]{0:T(1024)S(1)} %get-tuple-element.9, f32[1536]{0:T(1024)S(1)} %get-tuple-element.10, f32[1536]{0:T(1024)S(1)} %get-tuple-element.8, ...), kind=kOutput, calls=%fused_computation.21 | convolution fusion | flops 3282042880 | bytes 14716928 | tf_op jit(solution)/shard_map/dot_general | solution.py:41
  330.4 0.0 reduce-scatter.2.cloned.1.call-update
  330.4 29.5 %reduce-scatter.2.cloned.1.call-done = bf16[128,2048]{1,0:T(8,128)(2,1)} async-done(((bf16[512,2048]{1,0:T(8,128)(2,1)}), bf16[128,2048]{1,0:T(8,128)(2,1)}) %reduce-scatter.2.cloned.1.call-update) | async-done | bytes 524304 | tf_op jit(solution)/shard_map/reduce_scatter | solution.py:46
  359.9 1.2 convert_reduce_fusion
  361.1 1.3 fusion.18
  362.4 2.2 fusion.21
  (9 shorter events, 0.0 us)
Async XLA Ops:
  6.5 31.5 %copy-start = (bf16[128,2048]{1,0:T(8,128)(2,1)S(1)}, bf16[128,2048]{1,0:T(8,128)(2,1)}, u32[]{:S(2)}) copy-start(bf16[128,2048]{1,0:T(8,128)(2,1)} %param.8) | copy-start | bytes 1572868
  6.5 104.4 %all-gather.4.cloned.1.call-start = ((), (), s32[]{:S(2)}) async-start(), calls=%async_computation.1 | async-start | bytes 7077888 | tf_op jit(solution)/shard_map/all_gather | solution.py:36
  7.3 202.8 %all-gather.6.cloned.1.call-start = ((), (), s32[]{:S(2)}) async-start(), calls=%async_computation.2 | async-start | bytes 7077888 | tf_op jit(solution)/shard_map/all_gather | solution.py:37
  8.0 301.8 %all-gather.8.cloned.1.call-start = ((), (), s32[]{:S(2)}) async-start(), calls=%async_computation.3 | async-start | bytes 7077888 | tf_op jit(solution)/shard_map/all_gather | solution.py:43
  8.7 351.1 %reduce-scatter.2.cloned.1.call-start = ((), (), s32[]{:S(2)}) async-start(), calls=%async_computation.4 | async-start | bytes 2621440 | tf_op jit(solution)/shard_map/reduce_scatter | solution.py:46
  8.8 9.6 %collective-permute-start = (bf16[128,2048]{1,0:T(8,128)(2,1)}, bf16[128,2048]{1,0:T(8,128)(2,1)S(1)}, u32[]{:S(2)}, u32[]{:S(2)}) collective-permute-start(bf16[128,2048]{1,0:T(8,128)(2,1)} %param.8), channel_id=1, source_target_pairs={{0,1},{1,2},{2,3},{3,0},{4,5},{5,6},{6,7},{7,4},{8,9},{9,10},{10,1... | collective-permute-start | bytes 1572872 | tf_op jit(solution)/shard_map/ppermute | solution.py:11
  18.4 8.6 %collective-permute-start.1 = (bf16[128,2048]{1,0:T(8,128)(2,1)S(1)}, bf16[128,2048]{1,0:T(8,128)(2,1)S(1)}, u32[]{:S(2)}, u32[]{:S(2)}) collective-permute-start(bf16[128,2048]{1,0:T(8,128)(2,1)S(1)} %collective-permute-done), channel_id=1, source_target_pairs={{0,1},{1,2},{2,3},{3,0},{4,5},{5,6},{6,7},{7,4},{8,9},{9,10},{10,1... | collective-permute-start | bytes 1572872 | tf_op jit(solution)/shard_map/ppermute | solution.py:11
  27.0 8.6 %collective-permute-start.2 = (bf16[128,2048]{1,0:T(8,128)(2,1)S(1)}, bf16[128,2048]{1,0:T(8,128)(2,1)S(1)}, u32[]{:S(2)}, u32[]{:S(2)}) collective-permute-start(bf16[128,2048]{1,0:T(8,128)(2,1)S(1)} %collective-permute-done.1), channel_id=1, source_target_pairs={{0,1},{1,2},{2,3},{3,0},{4,5},{5,6},{6,7},{7,4},{8,9},{9,10},{10,1... | collective-permute-start | bytes 1572872 | tf_op jit(solution)/shard_map/ppermute | solution.py:11
  330.3 32.1 %copy-start.1 = (f32[2048]{0:T(1024)S(1)}, f32[2048]{0:T(1024)}, u32[]{:S(2)}) copy-start(f32[2048]{0:T(1024)} %param.15) | copy-start | bytes 24580
  330.3 32.1 %copy-start.2 = (f32[2048]{0:T(1024)S(1)}, f32[2048]{0:T(1024)}, u32[]{:S(2)}) copy-start(f32[2048]{0:T(1024)} %param.14) | copy-start | bytes 24580
Sparse Core Ops, SparseCore 0:
  9.5 101.4 all-gather.3
  113.1 96.8 all-gather.5
  212.1 97.6 all-gather.7
  330.5 29.3 reduce-scatter.1
